TPU v7x, 32 devices: a whole 2x2x4 slice. The times are simulated.
32 devices in a mesh: sp: 8 (over z, x), dp: 4 (over y, core).
Axes of the slice: x: 2, y: 2, z: 4, core: 2. Of those that a mesh axis runs over, the one named last changes fastest.
Arguments:
- residual_in: bfloat16 [4, 1024, 2048], P('dp', 'sp'), may hold values from -6 to 6
- ssm_input: bfloat16 [4, 1024, 2048], P('dp', 'sp'), may hold values from -6 to 6
- state_b: bfloat16 [4, 1024, 2048], P('dp', 'sp'), may hold values from -6 to 6
- state_c: bfloat16 [4, 1024, 2048], P('dp', 'sp'), may hold values from -6 to 6
- step_raw: bfloat16 [4, 1024, 64], P('dp', 'sp'), may hold values from -4 to 3
- gate_input: bfloat16 [4, 1024, 2048], P('dp', 'sp'), may hold values from -6 to 6
- conv_x: float32 [7, 2048], P(None, 'sp'), may hold values from -2 to 2
- conv_b: float32 [7, 2048], P(None, 'sp'), may hold values from -2 to 2
- conv_c: float32 [7, 2048], P(None, 'sp'), may hold values from -2 to 2
- decay_rate: float32 [2, 32], P(None, 'sp'), may hold values from 0 to 1, as said below
- mix_gain: float32 [2048], replicated, may hold values from 0.1 to 1.9
- out_weight: bfloat16 [2048, 2048], P('dp'), may hold values from -0.125 to 0.125
- ffn_gain: float32 [2048], replicated, may hold values from 0.1 to 1.9
- routing: int32 [4, 1024, 4], P('dp', 'sp'), may hold values from 0 to 31, all different within a row; in each aligned block of 128 rows (0 to 127, 128 to 255, ..., all dimensions but the last counted through in order) at most 32 rows name the same one
- route_weight: float32 [4, 1024, 4], P('dp', 'sp'), may hold values from 0.1 to 0.6
- gate_w: bfloat16 [32, 2048, 1024], P(('sp', 'dp')), may hold values from -60 to 60
- up_w: bfloat16 [32, 2048, 1024], P(('sp', 'dp')), may hold values from -60 to 60
- down_w: bfloat16 [32, 1024, 2048], P(('sp', 'dp')), may hold values from -0.1875 to 0.1875
Outputs:
- block_out: bfloat16 [4, 1024, 2048], P('dp', 'sp')
Inputs may be any that keep to these rules, and one draw needn't show every extreme that they name: `routing`: each row names 4 different experts; within the rows of one device no expert is named by more than 32 rows, a bound that some block reaches. `decay_rate`: Positive.
All inputs are finite; a program needn't handle non-finite values.
Results may differ from a plain program's by a relative error of at most 0.0082.
Values may be sent and summed in bfloat16 or wider, within the bound.
A program may use at most 128 MiB of HBM per device.

v0:
```python
import jax
import jax.numpy as jnp
from jax import lax
from jax.sharding import PartitionSpec as P

HEAD_DIM = 64
STATE = 128
BLOCK = 128
NORM_GROUPS = 4


highest = lax.Precision.HIGHEST
epsilon = 1e-05
clamp_limit = 7.0
sigmoid_slope = 1.702


def centred_conv(values, taps):
    half_width = taps.shape[0] // 2
    padded = jnp.pad(values, ((half_width, half_width), (0, 0)))
    total = jnp.zeros_like(values)
    for offset in range(taps.shape[0]):
        total = total + padded[offset : offset + values.shape[0]] * taps[offset]
    return total


def ssd_direction(signal, step_size, rates, write_map, read_map):
    length = signal.shape[0]
    head_count = signal.shape[1]
    head_width = signal.shape[2]
    group_count = write_map.shape[1]
    state_width = write_map.shape[2]
    per_group = head_count // group_count
    blocks = length // BLOCK
    scaled = (signal * step_size[..., None]).reshape(
        blocks, BLOCK, group_count, per_group, head_width
    )
    cumulative = jnp.cumsum(
        (-step_size * rates).reshape(blocks, BLOCK, group_count, per_group), axis=1
    )
    write_block = write_map.reshape(blocks, BLOCK, group_count, state_width)
    read_block = read_map.reshape(blocks, BLOCK, group_count, state_width)
    spread = cumulative[:, :, None] - cumulative[:, None]
    lower_mask = (lax.iota(jnp.int32, BLOCK)[:, None] >= lax.iota(jnp.int32, BLOCK)[None, :])[
        None, :, :, None, None
    ]
    weight_in = jnp.exp(jnp.where(lower_mask, spread, -jnp.inf))
    intersect = jnp.einsum("clgn,csgn->clsg", read_block, write_block, precision=highest)
    inside = jnp.einsum(
        "clsgk,csgkp->clgkp", intersect[..., None] * weight_in, scaled, precision=highest
    )
    to_end = jnp.exp(cumulative[:, -1:] - cumulative)
    states = jnp.einsum(
        "csgn,csgkp->cgkpn", write_block, scaled * to_end[..., None], precision=highest
    )
    carry_decay = jnp.exp(cumulative[:, -1])

    def advance(running, block_pair):
        block_state, factor = block_pair
        return (factor[..., None, None] * running + block_state, running)

    initial = jnp.zeros((group_count, per_group, head_width, state_width), jnp.float32)
    _, entering = lax.scan(advance, initial, (states, carry_decay))
    carried = (
        jnp.einsum("clgn,cgkpn->clgkp", read_block, entering, precision=highest)
        * jnp.exp(cumulative)[..., None]
    )
    return (inside + carried).reshape(length, head_count, head_width)


def both_ways(signal, steps_fwd, steps_bwd, rates, write_map, read_map):
    forward = ssd_direction(signal, steps_fwd, rates[0], write_map, read_map)
    backward = ssd_direction(
        jnp.flip(signal, 0),
        jnp.flip(steps_bwd, 0),
        rates[1],
        jnp.flip(write_map, 0),
        jnp.flip(read_map, 0),
    )
    return forward + jnp.flip(backward, 0)


def scale_rows(values, gains):
    return values * lax.rsqrt(jnp.mean(values * values, axis=-1, keepdims=True) + epsilon) * gains


def group_scale(values, gains):
    shaped = values.reshape(values.shape[:-1] + (NORM_GROUPS, values.shape[-1] // NORM_GROUPS))
    shaped = shaped * lax.rsqrt(jnp.mean(shaped * shaped, axis=-1, keepdims=True) + epsilon)
    return shaped.reshape(values.shape) * gains


def expert_apply(rows, gate_mat, up_mat, down_mat):
    gate_value = jnp.minimum(
        jnp.dot(rows, gate_mat, preferred_element_type=jnp.float32), clamp_limit
    )
    up_value = jnp.clip(
        jnp.dot(rows, up_mat, preferred_element_type=jnp.float32), -clamp_limit, clamp_limit
    )
    active = ((up_value + 1.0) * gate_value * jax.nn.sigmoid(sigmoid_slope * gate_value)).astype(
        jnp.bfloat16
    )
    return jnp.dot(active, down_mat, preferred_element_type=jnp.float32).astype(jnp.bfloat16)


def per_device(
    residual_in,
    ssm_input,
    state_b,
    state_c,
    step_raw,
    gate_input,
    conv_x,
    conv_b,
    conv_c,
    decay_rate,
    mix_gain,
    out_weight,
    ffn_gain,
    routing,
    route_weight,
    gate_w,
    up_w,
    down_w,
):
    signal_loc, write_loc, read_loc, step_loc = (
        lax.all_to_all(ssm_input, "sp", split_axis=2, concat_axis=1, tiled=True),
        lax.all_to_all(state_b, "sp", split_axis=2, concat_axis=1, tiled=True),
        lax.all_to_all(state_c, "sp", split_axis=2, concat_axis=1, tiled=True),
        lax.all_to_all(step_raw, "sp", split_axis=2, concat_axis=1, tiled=True),
    )
    length = signal_loc.shape[1]
    head_local = decay_rate.shape[1]
    signal = jax.nn.silu(centred_conv(signal_loc[0].astype(jnp.float32), conv_x)).reshape(
        length, head_local, HEAD_DIM
    )
    write_map = jax.nn.silu(centred_conv(write_loc[0].astype(jnp.float32), conv_b)).reshape(
        length, -1, STATE
    )
    read_map = jax.nn.silu(centred_conv(read_loc[0].astype(jnp.float32), conv_c)).reshape(
        length, -1, STATE
    )
    step_pair = jax.nn.softplus(step_loc[0].astype(jnp.float32).reshape(length, head_local, 2))
    mixed_heads = both_ways(
        signal, step_pair[..., 0], step_pair[..., 1], decay_rate, write_map, read_map
    )
    mixed_heads = mixed_heads.reshape(1, length, head_local * HEAD_DIM).astype(jnp.bfloat16)
    mixed_tokens = lax.all_to_all(mixed_heads, "sp", split_axis=1, concat_axis=2, tiled=True)
    token_count = residual_in.shape[1]
    model_width = residual_in.shape[2]
    gated = mixed_tokens[0].astype(jnp.float32) * jax.nn.silu(gate_input[0].astype(jnp.float32))
    mixed = group_scale(gated, mix_gain).astype(jnp.bfloat16)
    projected = jnp.dot(
        mixed,
        lax.all_gather(out_weight, "dp", axis=0, tiled=True),
        preferred_element_type=jnp.float32,
    )
    stream = residual_in[0].astype(jnp.float32) + projected
    ffn_input = scale_rows(stream, ffn_gain).astype(jnp.bfloat16)
    sp_count = lax.axis_size("sp")
    dp_count = lax.axis_size("dp")
    experts_all = sp_count * dp_count
    top_count = routing.shape[2]
    assigned = token_count * top_count
    capacity = 2 * assigned // experts_all
    flat_expert = routing.reshape(assigned)
    one_hot = (flat_expert[:, None] == lax.iota(jnp.int32, experts_all)[None, :]).astype(
        jnp.bfloat16
    )
    earlier = (
        lax.iota(jnp.int32, assigned)[:, None] > lax.iota(jnp.int32, assigned)[None, :]
    ).astype(jnp.bfloat16)
    before = jnp.dot(earlier, one_hot, preferred_element_type=jnp.float32)
    slot_index = jnp.sum(before * one_hot.astype(jnp.float32), axis=1).astype(jnp.int32)
    target = flat_expert * capacity + slot_index
    source_token = (
        jnp.zeros((experts_all * capacity,), jnp.int32)
        .at[target]
        .set(lax.iota(jnp.int32, assigned) // top_count)
    )
    filled = jnp.zeros((experts_all * capacity,), jnp.bool_).at[target].set(True)
    outgoing = jnp.where(filled[:, None], ffn_input[source_token], jnp.zeros((), jnp.bfloat16))
    arrived = lax.all_to_all(
        outgoing.reshape(experts_all, 1, capacity, model_width),
        ("sp", "dp"),
        split_axis=0,
        concat_axis=1,
        tiled=True,
    )
    served = expert_apply(arrived.reshape(-1, model_width), gate_w[0], up_w[0], down_w[0]).reshape(
        arrived.shape
    )
    returned = lax.all_to_all(served, ("sp", "dp"), split_axis=1, concat_axis=0, tiled=True)
    answers = returned.reshape(experts_all * capacity, model_width)[target].reshape(
        token_count, top_count, model_width
    )
    routed = jnp.sum(answers.astype(jnp.float32) * route_weight[0][:, :, None], axis=1)
    return (stream + routed).astype(jnp.bfloat16)[None]


def solution(mesh):
    return jax.shard_map(
        per_device,
        mesh=mesh,
        in_specs=(
            P("dp", "sp", None),
            P("dp", "sp", None),
            P("dp", "sp", None),
            P("dp", "sp", None),
            P("dp", "sp", None),
            P("dp", "sp", None),
            P(None, "sp"),
            P(None, "sp"),
            P(None, "sp"),
            P(None, "sp"),
            P(),
            P("dp", None),
            P(),
            P("dp", "sp", None),
            P("dp", "sp", None),
            P(("sp", "dp"), None, None),
            P(("sp", "dp"), None, None),
            P(("sp", "dp"), None, None),
        ),
        out_specs=P("dp", "sp", None),
        check_vma=False,
    )
```

profile of v0, /device:TPU:0, one launch (start us, length us, event | category | flops | bytes accessed | tf_op | source)
XLA Modules:
  0.0 593.2 jit_solution(14544832548649737198)
XLA Ops:
  9.2 7.3 %all-to-all-start.1 = ((bf16[8,2,512]{2,1,0:T(2,128)(2,1)}), bf16[8,2,512]{2,1,0:T(2,128)(2,1)S(1)}, u32[]{:S(2)}, u32[]{:S(2)}) async-start(bf16[8,2,512]{2,1,0:T(2,128)(2,1)} %reshape.329), calls=%async_computation.1 | async-start | bytes 32768 | tf_op jit(solution)/shard_map/all_to_all | solution.py:130
  25.2 11.5 %reduce.8 = bf16[2048,128]{1,0:T(8,128)(2,1)S(1)} reduce(bf16[2048,1,128]{2,1,0:T(2,128)(2,1)S(1)} %bitcast.256, bf16[]{:T(256)} %broadcast.189), dimensions={1}, to_apply=%bitcast.193.reduce_sub_computation | reduce | bytes 1048578
  38.4 11.5 %reduce.7 = bf16[2048,128]{1,0:T(8,128)(2,1)S(1)} reduce(bf16[2048,1,128]{2,1,0:T(2,128)(2,1)S(1)} %bitcast.257, bf16[]{:T(256)} %broadcast.189), dimensions={1}, to_apply=%bitcast.191.reduce_sub_computation | reduce | bytes 1048578
  51.6 11.8 %reduce.9 = bf16[2048,128]{1,0:T(8,128)(2,1)S(1)} reduce(bf16[2048,1,128]{2,1,0:T(2,128)(2,1)S(1)} %bitcast.258, bf16[]{:T(256)} %broadcast.189), dimensions={1}, to_apply=%bitcast.195.reduce_sub_computation | reduce | bytes 1048578
  64.4 6.0 %all-to-all-start = ((bf16[8,2,16384]{2,1,0:T(2,128)(2,1)}), bf16[8,2,16384]{2,1,0:T(2,128)(2,1)}, u32[]{:S(2)}, u32[]{:S(2)}) async-start(bf16[8,2,16384]{2,1,0:T(2,128)(2,1)} %reshape.333), calls=%async_computation | async-start | bytes 1048576 | tf_op jit(solution)/shard_map/all_to_all | solution.py:127
  71.8 47.4 %fusion.95 = f32[8,128,2,2]{3,0,1,2:T(8,128)S(1)} fusion(f32[8,128,2,2]{3,0,1,2:T(8,128)S(1)} %copy.202), kind=kOutput, calls=%fused_computation.155 | output fusion | flops 520192 | bytes 32768 | tf_op jit(solution)/shard_map/jit(cumsum)/reduce_window_sum | solution.py:38
  120.0 47.4 %fusion.94 = f32[8,128,2,2]{3,0,1,2:T(8,128)S(1)} fusion(f32[8,128,2,2]{3,0,1,2:T(8,128)S(1)} %copy.183), kind=kOutput, calls=%fused_computation.154 | output fusion | flops 520192 | bytes 32768 | tf_op jit(solution)/shard_map/jit(cumsum)/reduce_window_sum | solution.py:38
  170.5 6.0 %all-to-all-start.2 = ((bf16[8,2,16384]{2,1,0:T(2,128)(2,1)}), bf16[8,2,16384]{2,1,0:T(2,128)(2,1)}, u32[]{:S(2)}, u32[]{:S(2)}) async-start(bf16[8,2,16384]{2,1,0:T(2,128)(2,1)} %reshape.331), calls=%async_computation.2 | async-start | bytes 1048576 | tf_op jit(solution)/shard_map/all_to_all | solution.py:128
  190.0 6.2 %all-to-all-start.3 = ((bf16[8,2,16384]{2,1,0:T(2,128)(2,1)}), bf16[8,2,16384]{2,1,0:T(2,128)(2,1)}, u32[]{:S(2)}, u32[]{:S(2)}) async-start(bf16[8,2,16384]{2,1,0:T(2,128)(2,1)} %reshape.335), calls=%async_computation.3 | async-start | bytes 1048576 | tf_op jit(solution)/shard_map/all_to_all | solution.py:129
  203.0 6.8 %rev.20 = f32[1024,2,128]{2,0,1:T(8,128)S(1)} reverse(f32[1024,2,128]{2,0,1:T(8,128)} %copy_bitcast_fusion.1), dimensions={0} | reverse | bytes 2097152 | tf_op jit(solution)/shard_map/jit(_flip)/rev | solution.py:77
  218.3 6.2 %copy_bitcast_fusion = f32[1024,2,128]{2,0,1:T(8,128)} fusion(f32[256]{0:T(256)} %bitcast.284, f32[256]{0:T(256)} %bitcast.286, f32[256]{0:T(256)S(1)} %bitcast.276, f32[1024,256]{1,0:T(8,128)} %bitcast.240, f32[256]{0:T(256)S(1)} %bitcast.278, f32[256]{0:T(256)S(1)} %bitcast.280, f32[256]{0:T(256)} %bitcast.282, f32[256]{0:T(256)S(1)} %bitcast.274), kind=kLoop, calls=%fused_computation.43 | loop fusion | flops 4456448 | bytes 2104320 | tf_op jit(solution)/shard_map/reshape | solution.py:140
  224.5 6.8 %rev.21 = f32[1024,2,128]{2,0,1:T(8,128)S(1)} reverse(f32[1024,2,128]{2,0,1:T(8,128)} %copy_bitcast_fusion), dimensions={0} | reverse | bytes 2097152 | tf_op jit(solution)/shard_map/jit(_flip)/rev | solution.py:78
  241.9 18.6 %while.27 = (s32[]{:T(128)}, f32[2,2,64,128]{3,2,1,0:T(8,128)S(1)}, f32[8,2,2,64,128]{4,3,2,1,0:T(8,128)}, f32[8,2,2]{2,1,0:T(2,128)}, f32[8,2,2,64,128]{4,3,2,1,0:T(8,128)}, /*index=5*/s32[]{:T(128)}, s32[]{:T(128)}) while((s32[]{:T(128)}, f32[2,2,64,128]{3,2,1,0:T(8,128)S(1)}, f32[8,2,2,64,128]{4,3,2,1,0:T(8,128)}, ...), condition=%wide.region_5.6_spmd.clone, body=%wide.region_4.5_spmd.clone.sunk | while | flops 131075 | bytes 656016 | solution.py:63
  271.5 5.6 rev.22
  293.4 13.7 %while.26 = (s32[]{:T(128)}, f32[2,2,64,128]{3,2,1,0:T(8,128)S(1)}, f32[8,2,2,64,128]{4,3,2,1,0:T(8,128)S(1)}, f32[8,2,2]{2,1,0:T(2,128)}, f32[8,2,2,64,128]{4,3,2,1,0:T(8,128)}, /*index=5*/s32[]{:T(128)}, s32[]{:T(128)}) while((s32[]{:T(128)}, f32[2,2,64,128]{3,2,1,0:T(8,128)S(1)}, f32[8,2,2,64,128]{4,3,2,1,0:T(8,128)S(1)}, ...), condition=%wide.region_2.3_spmd.clone, body=%wide.region_1.2_spmd.clone.sunk | while | flops 131075 | bytes 655508 | solution.py:63
  309.4 5.6 fusion.24
  321.5 6.0 %all-to-all-start.4 = ((bf16[8,2,16384]{2,1,0:T(2,128)(2,1)}), bf16[8,2,16384]{2,1,0:T(2,128)(2,1)S(1)}, u32[]{:S(2)}, u32[]{:S(2)}) async-start(bf16[8,2,16384]{2,1,0:T(2,128)(2,1)} %reshape.337), calls=%async_computation.4 | async-start | bytes 1048576 | tf_op jit(solution)/shard_map/all_to_all | solution.py:148
  334.1 5.7 all-to-all-done.4
  348.9 6.0 %gather_fusion = bf16[1024,2048]{1,0:T(8,128)(2,1)} fusion(bf16[128,2048]{1,0:T(8,128)(2,1)S(1)} %multiply_convert_fusion.1, s32[1024]{0:T(1024)S(1)} %fusion.78), kind=kCustom, calls=%fused_computation | custom fusion | bytes 8392704 | tf_op jit(solution)/shard_map/gather | solution.py:182
  357.5 97.6 %all_to_all.28 = bf16[32,1,32,2048]{3,2,1,0:T(8,128)(2,1)S(1)} all-to-all(bf16[32,1,32,2048]{3,2,1,0:T(8,128)(2,1)S(1)} %broadcast_select_fusion), channel_id=1, replica_groups=mesh['sp'=8,'dp'=4] {'sp','dp'}, dimensions={0} | all-to-all | bytes 8388608 | tf_op jit(solution)/shard_map/all_to_all | solution.py:183
  459.7 5.7 multiply_convert_fusion
  465.3 6.1 %fusion.6 = bf16[1024,2048]{1,0:T(8,128)(2,1)} fusion(bf16[1024,1024]{1,0:T(8,128)(2,1)S(1)} %multiply_convert_fusion, bf16[1,1024,2048]{2,1,0:T(8,128)(2,1)S(1)} %copy-done.35), kind=kOutput, calls=%fused_computation.19 | convolution fusion | flops 4297064448 | bytes 10485760 | tf_op jit(solution)/shard_map/dot_general | solution.py:103
  475.6 94.1 %all-to-all-done.6 = bf16[1,32,32,2048]{3,2,0,1:T(8,128)(2,1)} async-done(((bf16[1,32,32,2048]{3,2,0,1:T(8,128)(2,1)}), bf16[1,32,32,2048]{3,2,0,1:T(8,128)(2,1)}, u32[]{:S(2)}, u32[]{:S(2)}) %all-to-all-start.6) | async-done | bytes 4194336 | tf_op jit(solution)/shard_map/all_to_all | solution.py:193
  569.7 7.1 %gather_fusion.1 = bf16[512,2048]{1,0:T(8,128)(2,1)S(1)} fusion(bf16[1024,2048]{1,0:T(8,128)(2,1)} %bitcast.69, s32[1024]{0:T(1024)S(1)} %pad_clamp_fusion), kind=kCustom, calls=%fused_computation.1 | custom fusion | bytes 4196352 | tf_op jit(solution)/shard_map/gather | solution.py:194
  (254 shorter events, 163.4 us)
Async XLA Ops:
  6.5 31.1 %copy-start.7 = (bf16[1,128,2048]{2,1,0:T(8,128)(2,1)S(1)}, bf16[1,128,2048]{2,1,0:T(8,128)(2,1)}, u32[]{:S(2)}) copy-start(bf16[1,128,2048]{2,1,0:T(8,128)(2,1)} %param.24) | copy-start | bytes 1572868
  9.2 55.2 %all-to-all-start.1 = ((bf16[8,2,512]{2,1,0:T(2,128)(2,1)}), bf16[8,2,512]{2,1,0:T(2,128)(2,1)S(1)}, u32[]{:S(2)}, u32[]{:S(2)}) async-start(bf16[8,2,512]{2,1,0:T(2,128)(2,1)} %reshape.329), calls=%async_computation.1 | async-start | bytes 32768 | tf_op jit(solution)/shard_map/all_to_all | solution.py:130
  16.5 327.5 %all-gather.2.cloned.1.call-start = ((), (), s32[]{:S(2)}) async-start(), calls=%async_computation.7 | async-start | bytes 10485760 | tf_op jit(solution)/shard_map/all_gather | solution.py:155
  22.7 28.1 %copy-start.8 = (bf16[1,128,2048]{2,1,0:T(8,128)(2,1)S(1)}, bf16[1,128,2048]{2,1,0:T(8,128)(2,1)}, u32[]{:S(2)}) copy-start(bf16[1,128,2048]{2,1,0:T(8,128)(2,1)} %param.25) | copy-start | bytes 1572868
  64.4 106.2 %all-to-all-start = ((bf16[8,2,16384]{2,1,0:T(2,128)(2,1)}), bf16[8,2,16384]{2,1,0:T(2,128)(2,1)}, u32[]{:S(2)}, u32[]{:S(2)}) async-start(bf16[8,2,16384]{2,1,0:T(2,128)(2,1)} %reshape.333), calls=%async_computation | async-start | bytes 1048576 | tf_op jit(solution)/shard_map/all_to_all | solution.py:127
  170.5 19.5 %all-to-all-start.2 = ((bf16[8,2,16384]{2,1,0:T(2,128)(2,1)}), bf16[8,2,16384]{2,1,0:T(2,128)(2,1)}, u32[]{:S(2)}, u32[]{:S(2)}) async-start(bf16[8,2,16384]{2,1,0:T(2,128)(2,1)} %reshape.331), calls=%async_computation.2 | async-start | bytes 1048576 | tf_op jit(solution)/shard_map/all_to_all | solution.py:128
  190.0 19.9 %all-to-all-start.3 = ((bf16[8,2,16384]{2,1,0:T(2,128)(2,1)}), bf16[8,2,16384]{2,1,0:T(2,128)(2,1)}, u32[]{:S(2)}, u32[]{:S(2)}) async-start(bf16[8,2,16384]{2,1,0:T(2,128)(2,1)} %reshape.335), calls=%async_computation.3 | async-start | bytes 1048576 | tf_op jit(solution)/shard_map/all_to_all | solution.py:129
  200.2 15.5 %copy-start = (f32[1,8,128,256]{3,2,1,0:T(8,128)}, f32[1,8,128,256]{3,2,1,0:T(8,128)S(1)}, u32[]{:S(2)}) copy-start(f32[1,8,128,256]{3,2,1,0:T(8,128)S(1)} %copy.175) | copy-start | bytes 3145732
  203.0 15.3 %copy-start.10 = (f32[1,256]{1,0:T(1,128)S(1)}, f32[1,256]{1,0:T(1,128)}, u32[]{:S(2)}) copy-start(f32[1,256]{1,0:T(1,128)} %get-tuple-element.177) | copy-start | bytes 3076
  203.0 15.3 %copy-start.11 = (f32[1,256]{1,0:T(1,128)S(1)}, f32[1,256]{1,0:T(1,128)}, u32[]{:S(2)}) copy-start(f32[1,256]{1,0:T(1,128)} %get-tuple-element.178) | copy-start | bytes 3076
  203.0 15.3 %copy-start.12 = (f32[1,256]{1,0:T(1,128)S(1)}, f32[1,256]{1,0:T(1,128)}, u32[]{:S(2)}) copy-start(f32[1,256]{1,0:T(1,128)} %get-tuple-element.179) | copy-start | bytes 3076
  203.0 15.3 %copy-start.13 = (f32[1,256]{1,0:T(1,128)S(1)}, f32[1,256]{1,0:T(1,128)}, u32[]{:S(2)}) copy-start(f32[1,256]{1,0:T(1,128)} %get-tuple-element.180) | copy-start | bytes 3076
  240.8 23.3 %copy-start.3 = (f32[32,8,8,128]{3,2,1,0:T(8,128)S(1)}, f32[32,8,8,128]{3,2,1,0:T(8,128)}, u32[]{:S(2)}) copy-start(f32[32,8,8,128]{3,2,1,0:T(8,128)} %copy.245) | copy-start | bytes 3145732
  269.6 8.7 %copy-start.1 = (f32[1,8,128,256]{3,2,1,0:T(8,128)S(1)}, f32[1,8,128,256]{3,2,1,0:T(8,128)}, u32[]{:S(2)}) copy-start(f32[1,8,128,256]{3,2,1,0:T(8,128)} %copy-done) | copy-start | bytes 3145732
  269.6 8.7 %copy-start.19 = (f32[1,256]{1,0:T(1,128)S(1)}, f32[1,256]{1,0:T(1,128)}, u32[]{:S(2)}) copy-start(f32[1,256]{1,0:T(1,128)} %get-tuple-element.191) | copy-start | bytes 3076
  269.6 8.7 %copy-start.21 = (f32[1,256]{1,0:T(1,128)S(1)}, f32[1,256]{1,0:T(1,128)}, u32[]{:S(2)}) copy-start(f32[1,256]{1,0:T(1,128)} %get-tuple-element.192) | copy-start | bytes 3076
  269.6 8.7 %copy-start.23 = (f32[1,256]{1,0:T(1,128)S(1)}, f32[1,256]{1,0:T(1,128)}, u32[]{:S(2)}) copy-start(f32[1,256]{1,0:T(1,128)} %get-tuple-element.193) | copy-start | bytes 3076
  293.3 16.1 %copy-start.6 = (f32[8,128,2,2,64]{1,0,4,3,2:T(8,128)S(1)}, f32[8,128,2,2,64]{1,0,4,3,2:T(8,128)}, u32[]{:S(2)}) copy-start(f32[8,128,2,2,64]{1,0,4,3,2:T(8,128)} %get-tuple-element.170) | copy-start | bytes 3145732
  315.9 11.6 %copy-start.9 = (bf16[1,128,2048]{2,1,0:T(8,128)(2,1)S(1)}, bf16[1,128,2048]{2,1,0:T(8,128)(2,1)}, u32[]{:S(2)}) copy-start(bf16[1,128,2048]{2,1,0:T(8,128)(2,1)} %param.27) | copy-start | bytes 1572868
  315.9 12.1 %copy-start.31 = (s32[1,128,4]{1,2,0:T(4,128)S(1)}, s32[1,128,4]{1,2,0:T(4,128)}, u32[]{:S(2)}) copy-start(s32[1,128,4]{1,2,0:T(4,128)} %param.35) | copy-start | bytes 6148
  321.5 18.2 %all-to-all-start.4 = ((bf16[8,2,16384]{2,1,0:T(2,128)(2,1)}), bf16[8,2,16384]{2,1,0:T(2,128)(2,1)S(1)}, u32[]{:S(2)}, u32[]{:S(2)}) async-start(bf16[8,2,16384]{2,1,0:T(2,128)(2,1)} %reshape.337), calls=%async_computation.4 | async-start | bytes 1048576 | tf_op jit(solution)/shard_map/all_to_all | solution.py:148
  328.3 15.3 %copy-start.29 = (f32[2048]{0:T(1024)S(1)}, f32[2048]{0:T(1024)}, u32[]{:S(2)}) copy-start(f32[2048]{0:T(1024)} %param.32) | copy-start | bytes 24580
  357.5 97.6 %copy-start.33 = (bf16[1,2048,1024]{2,1,0:T(8,128)(2,1)S(1)}, bf16[1,2048,1024]{2,1,0:T(8,128)(2,1)}, u32[]{:S(2)}) copy-start(bf16[1,2048,1024]{2,1,0:T(8,128)(2,1)} %param.37) | copy-start | bytes 12582916
  471.5 98.2 %all-to-all-start.6 = ((bf16[1,32,32,2048]{3,2,0,1:T(8,128)(2,1)}), bf16[1,32,32,2048]{3,2,0,1:T(8,128)(2,1)}, u32[]{:S(2)}, u32[]{:S(2)}) async-start(bf16[1,32,32,2048]{3,2,0,1:T(8,128)(2,1)} %bitcast.249), calls=%async_computation.6 | async-start | bytes 8388608 | tf_op jit(solution)/shard_map/all_to_all | solution.py:193
  (19 other events, 126.1 us)
Sparse Core Ops, SparseCore 0:
  18.9 59.6 all-gather.1
where the time goes:
time: 604 us; the launch traced here: 593 us
  other arithmetic  188 us (31%)
  local copies, waits for them, and re-layouts  107 us (18%)
  waiting for transfers between devices  101 us (17%)
  blocking collectives  97.6 us (16%)
  matrix products  49.4 us (8%)
  starting transfers between devices  35.4 us (6%)
  between operations  14.5 us (2%)
    all_to_all x1, blocking collectives, per_device(): lax.all_to_all(outgoing.reshape(experts_all, 1, capacity, model_width), (...  97.6 us
    another operation x2, other arithmetic, ssd_direction(): jnp.cumsum((-step_size * rates).reshape(blocks, BLOCK, group_count, per_g...  94.9 us
    all_to_all x1, waiting for transfers between devices, per_device(): lax.all_to_all(served, ('sp', 'dp'), split_axis=1, concat_axis=0, tiled=T...  94.1 us
    unnamed x8, other arithmetic  39.5 us
    unnamed x95, local copies, waits for them, and re-layouts  22.3 us
    add x16, other arithmetic, advance(): return (factor[..., None, None] * running + block_state, running)  15.7 us
  transfers between devices with their start and end apart: 7, of which 3 were waited for; matrix products, arithmetic and copies ran while one was open for 50% of the time, Pallas kernels for 0%

commit v1 on v0

v1 whole, which is shorter than its diff:
```python
import functools

import jax
import jax.numpy as jnp
from jax import lax
from jax.experimental import pallas as pl
from jax.experimental.pallas import tpu as pltpu
from jax.sharding import PartitionSpec as P

HEAD_DIM = 64
STATE = 128
BLOCK = 128
NORM_GROUPS = 4
MESH = pl.DeviceIdType.MESH

highest = lax.Precision.HIGHEST
epsilon = 1e-05
clamp_limit = 7.0
sigmoid_slope = 1.702


def greet(peers):
    barrier = pltpu.get_barrier_semaphore()
    for peer in peers:
        pl.semaphore_signal(barrier, inc=1, device_id=peer, device_id_type=MESH)
    pl.semaphore_wait(barrier, len(peers))


def to_heads_kernel(n, *refs):
    srcs, dsts = refs[:4], refs[4:8]
    bounce, step_bounce, send, recv, local = refs[8:]
    me = lax.axis_index("sp")
    rows = srcs[0].shape[0]
    width = dsts[0].shape[1]
    peers = [lax.rem(me + i, n) for i in range(1, n)]
    greet([{"sp": peer} for peer in peers])
    copies = []
    mine = pl.ds(pl.multiple_of(me * rows, rows), rows)
    for i, peer in enumerate(peers):
        for k in range(4):
            if k < 3:
                part = srcs[k].at[:, pl.ds(pl.multiple_of(peer * width, width), width)]
                there = dsts[k].at[mine, :]
            else:
                part = srcs[k]
                there = dsts[k].at[mine, :]
            copy = pltpu.make_async_remote_copy(
                src_ref=part,
                dst_ref=there,
                send_sem=send.at[i, k],
                recv_sem=recv.at[i, k],
                device_id={"sp": peer},
                device_id_type=MESH,
            )
            copy.start()
            copies.append(copy)
    own = [srcs[k].at[:, pl.ds(pl.multiple_of(me * width, width), width)] for k in range(3)]
    own.append(srcs[3])
    slots = [bounce.at[k] for k in range(3)] + [step_bounce]
    first = [pltpu.make_async_copy(own[k], slots[k], local.at[0, k]) for k in range(4)]
    second = [
        pltpu.make_async_copy(slots[k], dsts[k].at[mine, :], local.at[1, k]) for k in range(4)
    ]
    for k in range(4):
        first[k].start()
    for k in range(4):
        first[k].wait()
        second[k].start()
    for k in range(4):
        second[k].wait()
    for copy in copies:
        copy.wait()


def to_heads(n, arrays, steps):
    rows, full = arrays[0].shape
    width = full // n
    wide = jax.ShapeDtypeStruct((rows * n, width), arrays[0].dtype)
    step_out = jax.ShapeDtypeStruct((rows * n, steps.shape[1]), steps.dtype)
    anywhere = pl.BlockSpec(memory_space=pl.ANY)
    return pl.pallas_call(
        functools.partial(to_heads_kernel, n),
        out_shape=(wide, wide, wide, step_out),
        in_specs=[anywhere] * 4,
        out_specs=(anywhere,) * 4,
        scratch_shapes=[
            pltpu.VMEM((3, rows, width), arrays[0].dtype),
            pltpu.VMEM(steps.shape, steps.dtype),
            pltpu.SemaphoreType.DMA((n - 1, 4)),
            pltpu.SemaphoreType.DMA((n - 1, 4)),
            pltpu.SemaphoreType.DMA((2, 4)),
        ],
        compiler_params=pltpu.CompilerParams(collective_id=1, has_side_effects=True),
        name="to_heads",
    )(*arrays, steps)


def to_tokens_kernel(n, src, dst, bounce, send, recv, local):
    me = lax.axis_index("sp")
    rows = dst.shape[0]
    width = src.shape[1]
    peers = [lax.rem(me + i, n) for i in range(1, n)]
    greet([{"sp": peer} for peer in peers])
    there = dst.at[:, pl.ds(pl.multiple_of(me * width, width), width)]
    copies = []
    for i, peer in enumerate(peers):
        copy = pltpu.make_async_remote_copy(
            src_ref=src.at[pl.ds(pl.multiple_of(peer * rows, rows), rows), :],
            dst_ref=there,
            send_sem=send.at[i],
            recv_sem=recv.at[i],
            device_id={"sp": peer},
            device_id_type=MESH,
        )
        copy.start()
        copies.append(copy)
    first = pltpu.make_async_copy(
        src.at[pl.ds(pl.multiple_of(me * rows, rows), rows), :], bounce, local.at[0]
    )
    first.start()
    first.wait()
    second = pltpu.make_async_copy(bounce, there, local.at[1])
    second.start()
    second.wait()
    for copy in copies:
        copy.wait()


def to_tokens(n, heads):
    length, width = heads.shape
    rows = length // n
    anywhere = pl.BlockSpec(memory_space=pl.ANY)
    return pl.pallas_call(
        functools.partial(to_tokens_kernel, n),
        out_shape=jax.ShapeDtypeStruct((rows, n * width), heads.dtype),
        in_specs=[anywhere],
        out_specs=anywhere,
        scratch_shapes=[
            pltpu.VMEM((rows, width), heads.dtype),
            pltpu.SemaphoreType.DMA((n - 1,)),
            pltpu.SemaphoreType.DMA((n - 1,)),
            pltpu.SemaphoreType.DMA((2,)),
        ],
        compiler_params=pltpu.CompilerParams(collective_id=2, has_side_effects=True),
        name="to_tokens",
    )(heads)


def swap_half_kernel(half, dp_count, src, dst, bounce, send, recv, local):
    n = half * dp_count
    first_sp = lax.axis_index("sp") // half * half
    me = lax.rem(lax.axis_index("sp"), half) * dp_count + lax.axis_index("dp")

    def place(peer):
        return {"sp": first_sp + peer // dp_count, "dp": lax.rem(peer, dp_count)}

    barrier = pltpu.get_barrier_semaphore()

    def call(i, carry):
        peer = lax.rem(me + i, n)
        pl.semaphore_signal(barrier, inc=1, device_id=place(peer), device_id_type=MESH)
        return carry

    lax.fori_loop(1, n, call, 0)
    pl.semaphore_wait(barrier, n - 1)

    def remote(i):
        peer = lax.rem(me + i, n)
        return pltpu.make_async_remote_copy(
            src_ref=src.at[peer],
            dst_ref=dst.at[me],
            send_sem=send.at[i - 1],
            recv_sem=recv.at[i - 1],
            device_id=place(peer),
            device_id_type=MESH,
        )

    def begin(i, carry):
        remote(i).start()
        return carry

    lax.fori_loop(1, n, begin, 0)
    first = pltpu.make_async_copy(src.at[me], bounce, local.at[0])
    first.start()
    first.wait()
    second = pltpu.make_async_copy(bounce, dst.at[me], local.at[1])
    second.start()
    second.wait()

    def finish(i, carry):
        remote(i).wait()
        return carry

    lax.fori_loop(1, n, finish, 0)


def swap_half(half, dp_count, rows, identity):
    n = half * dp_count
    anywhere = pl.BlockSpec(memory_space=pl.ANY)
    return pl.pallas_call(
        functools.partial(swap_half_kernel, half, dp_count),
        out_shape=jax.ShapeDtypeStruct(rows.shape, rows.dtype),
        in_specs=[anywhere],
        out_specs=anywhere,
        scratch_shapes=[
            pltpu.VMEM(rows.shape[1:], rows.dtype),
            pltpu.SemaphoreType.DMA((n - 1,)),
            pltpu.SemaphoreType.DMA((n - 1,)),
            pltpu.SemaphoreType.DMA((2,)),
        ],
        compiler_params=pltpu.CompilerParams(collective_id=identity, has_side_effects=True),
        cost_estimate=pl.CostEstimate(flops=10**11, bytes_accessed=rows.size * 4, transcendentals=0),
        name="swap_half_%d" % identity,
    )(rows)


def mixer_kernel(
    x_ref, b_ref, c_ref, tx_ref, tb_ref, tc_ref, st_ref, stt_ref, rate_ref, ratet_ref,
    o_ref, pad, reads, inside_ref, fade_f, fade_b, sums, carry,
):
    length = x_ref.shape[0]
    lanes = x_ref.shape[1]
    blocks = length // BLOCK
    per_group = st_ref.shape[2] // 2
    taps = tx_ref.shape[0]
    half = taps // 2
    f32, bf16 = jnp.float32, jnp.bfloat16
    for k, ref in enumerate((x_ref, b_ref, c_ref)):
        pad[k, 0:8, :] = jnp.zeros((8, lanes), f32)
        pad[k, length + 8 : length + 16, :] = jnp.zeros((8, lanes), f32)
        pad[k, 8 : length + 8, :] = ref[...].astype(f32)

    def conv(k, taps_ref, base):
        total = None
        for j in range(taps):
            term = pad[k, base + 8 - half + j : base + 8 - half + j + BLOCK, :] * taps_ref[j : j + 1, :]
            total = term if total is None else total + term
        return total * jax.nn.sigmoid(total)

    def softplus(v):
        return jnp.maximum(v, 0.0) + jnp.log(1.0 + jnp.exp(-jnp.abs(v)))

    li = lax.broadcasted_iota(jnp.int32, (BLOCK, BLOCK), 0)
    si = lax.broadcasted_iota(jnp.int32, (BLOCK, BLOCK), 1)
    at_or_after = li >= si
    lower = jnp.where(at_or_after, 1.0, 0.0).astype(f32)
    upper = jnp.where(si >= li, 1.0, 0.0).astype(f32)
    lane_head = lax.broadcasted_iota(jnp.int32, (1, lanes), 1) // HEAD_DIM

    def spread_heads(columns):
        out = columns[0]
        for h in range(1, per_group):
            out = jnp.where(lane_head == h, columns[h], out)
        return jnp.broadcast_to(out, (out.shape[0], lanes))

    for c in range(blocks):
        base = c * BLOCK
        rows = slice(base, base + BLOCK)
        x = conv(0, tx_ref, base)
        write = conv(1, tb_ref, base).astype(bf16)
        read = conv(2, tc_ref, base).astype(bf16)
        reads[rows, :] = read
        dt = softplus(st_ref[0, rows, :])
        dtt = softplus(stt_ref[0, :, rows])
        a = dt * rate_ref[0]
        at = dtt * ratet_ref[0]
        inc = jnp.dot(lower, a, precision=highest, preferred_element_type=f32)
        inct = jnp.dot(at, upper, precision=highest, preferred_element_type=f32)
        exc = inc - a
        exct = inct - at
        tot = inc[BLOCK - 1 : BLOCK, :]
        scores = lax.dot_general(
            read, write, (((1,), (1,)), ((), ())), preferred_element_type=f32
        )
        inside = None
        xb = x.astype(bf16)
        for h in range(per_group):
            f, b = 2 * h, 2 * h + 1
            power = jnp.where(
                at_or_after,
                inct[f : f + 1, :] - inc[:, f : f + 1],
                exc[:, b : b + 1] - exct[b : b + 1, :],
            )
            df, db = dtt[f : f + 1, :], dtt[b : b + 1, :]
            scale = jnp.where(li > si, df, jnp.where(li == si, df + db, db))
            weights = (scores * jnp.exp(power) * scale).astype(bf16)
            xh = jnp.where(lane_head == h, x, 0.0).astype(bf16)
            term = jnp.dot(weights, xh, preferred_element_type=f32)
            inside = term if inside is None else inside + term
        inside_ref[rows, :] = inside
        heads = range(per_group)
        fwd = [inc[:, 2 * h : 2 * h + 1] for h in heads]
        bwd = [exc[:, 2 * h + 1 : 2 * h + 2] for h in heads]
        tot_f = [tot[:, 2 * h : 2 * h + 1] for h in heads]
        tot_b = [tot[:, 2 * h + 1 : 2 * h + 2] for h in heads]
        wf = spread_heads([dt[:, 2 * h : 2 * h + 1] * jnp.exp(fwd[h] - tot_f[h]) for h in heads])
        wb = spread_heads([dt[:, 2 * h + 1 : 2 * h + 2] * jnp.exp(-bwd[h]) for h in heads])
        fade_f[rows, :] = spread_heads([jnp.exp(-fwd[h]) for h in heads])
        fade_b[rows, :] = spread_heads([jnp.exp(bwd[h] - tot_b[h]) for h in heads])
        both = jnp.concatenate([(x * wf).astype(bf16), (x * wb).astype(bf16)], axis=1)
        sums[c] = lax.dot_general(
            write, both, (((0,), (0,)), ((), ())), preferred_element_type=f32
        )
        carry[c : c + 1, :] = jnp.concatenate(
            [
                spread_heads([jnp.exp(-tot_f[h]) for h in heads]),
                spread_heads([jnp.exp(-tot_b[h]) for h in heads]),
            ],
            axis=1,
        )

    state = jnp.zeros((sums.shape[1], lanes), f32)
    for c in range(blocks):
        own = sums[c, :, 0:lanes]
        sums[c, :, 0:lanes] = state
        state = carry[c : c + 1, 0:lanes] * state + own
    state = jnp.zeros((sums.shape[1], lanes), f32)
    for c in reversed(range(blocks)):
        own = sums[c, :, lanes : 2 * lanes]
        sums[c, :, lanes : 2 * lanes] = state
        state = carry[c : c + 1, lanes : 2 * lanes] * state + own
    for c in range(blocks):
        rows = slice(c * BLOCK, (c + 1) * BLOCK)
        moved = jnp.dot(reads[rows, :], sums[c].astype(bf16), preferred_element_type=f32)
        total = (
            inside_ref[rows, :]
            + moved[:, 0:lanes] * fade_f[rows, :]
            + moved[:, lanes : 2 * lanes] * fade_b[rows, :]
        )
        o_ref[rows, :] = total.astype(o_ref.dtype)


def mixer(signal, write, read, conv_x, conv_b, conv_c, steps, rates):
    length, width = signal.shape
    groups = write.shape[1] // STATE
    lanes = width // groups
    columns = steps.shape[1] // groups
    taps = conv_x.shape[0]
    blocks = length // BLOCK
    st = steps.astype(jnp.float32).reshape(length, groups, columns).transpose(1, 0, 2)
    stt = st.transpose(0, 2, 1)
    rate = rates.T.reshape(groups, 1, columns)
    ratet = rates.T.reshape(groups, columns, 1)
    wide = pl.BlockSpec((length, lanes), lambda g: (0, g))
    state = pl.BlockSpec((length, STATE), lambda g: (0, g))
    tap_x = pl.BlockSpec((taps, lanes), lambda g: (0, g))
    tap_s = pl.BlockSpec((taps, STATE), lambda g: (0, g))

    def whole(shape):
        return pl.BlockSpec((1,) + shape, lambda g: (g, 0, 0))

    f32 = jnp.float32
    return pl.pallas_call(
        mixer_kernel,
        grid=(groups,),
        out_shape=jax.ShapeDtypeStruct((length, width), jnp.bfloat16),
        in_specs=[
            wide, state, state, tap_x, tap_s, tap_s,
            whole((length, columns)), whole((columns, length)),
            whole((1, columns)), whole((columns, 1)),
        ],
        out_specs=wide,
        scratch_shapes=[
            pltpu.VMEM((3, length + 16, lanes), f32),
            pltpu.VMEM((length, STATE), jnp.bfloat16),
            pltpu.VMEM((length, lanes), f32),
            pltpu.VMEM((length, lanes), f32),
            pltpu.VMEM((length, lanes), f32),
            pltpu.VMEM((blocks, STATE, 2 * lanes), f32),
            pltpu.VMEM((blocks, 2 * lanes), f32),
        ],
        compiler_params=pltpu.CompilerParams(vmem_limit_bytes=40 * 1024 * 1024),
        cost_estimate=pl.CostEstimate(
            flops=40 * 10**9, bytes_accessed=4 * length * width * 2, transcendentals=0
        ),
        name="mixer",
    )(signal, write, read, conv_x, conv_b, conv_c, st, stt, rate, ratet)


def scale_rows(values, gains):
    return values * lax.rsqrt(jnp.mean(values * values, axis=-1, keepdims=True) + epsilon) * gains


def group_scale(values, gains):
    shaped = values.reshape(values.shape[:-1] + (NORM_GROUPS, values.shape[-1] // NORM_GROUPS))
    shaped = shaped * lax.rsqrt(jnp.mean(shaped * shaped, axis=-1, keepdims=True) + epsilon)
    return shaped.reshape(values.shape) * gains


def expert_apply(rows, gate_mat, up_mat, down_mat):
    gate_value = jnp.minimum(
        jnp.dot(rows, gate_mat, preferred_element_type=jnp.float32), clamp_limit
    )
    up_value = jnp.clip(
        jnp.dot(rows, up_mat, preferred_element_type=jnp.float32), -clamp_limit, clamp_limit
    )
    active = ((up_value + 1.0) * gate_value * jax.nn.sigmoid(sigmoid_slope * gate_value)).astype(
        jnp.bfloat16
    )
    return jnp.dot(active, down_mat, preferred_element_type=jnp.float32).astype(jnp.bfloat16)


def gather_rows(weight, count):
    parts = {0: weight}
    step = count // 2
    while step >= 1:
        pairs = [(d, d ^ step) for d in range(count)]
        for offset, block in list(parts.items()):
            parts[offset ^ step] = lax.ppermute(block, "dp", pairs)
        step //= 2
    return parts


def per_device(
    residual_in, ssm_input, state_b, state_c, step_raw, gate_input, conv_x, conv_b, conv_c,
    decay_rate, mix_gain, out_weight, ffn_gain, routing, route_weight, gate_w, up_w, down_w,
):
    sp_count = lax.axis_size("sp")
    dp_count = lax.axis_size("dp")
    bf16, f32 = jnp.bfloat16, jnp.float32
    half = sp_count // 2
    near = half * dp_count
    mirror = [(i, (i + half) % sp_count) for i in range(sp_count)]
    first_expert = lax.axis_index("sp") // half * near
    far_routing = lax.ppermute(routing[0], "sp", mirror)
    far_weight = lax.ppermute(route_weight[0], "sp", mirror)
    parts = gather_rows(out_weight, dp_count)
    signal, write, read, steps = to_heads(
        sp_count, (ssm_input[0], state_b[0], state_c[0]), step_raw[0]
    )
    columns = steps.shape[1] // sp_count
    steps = lax.dynamic_slice_in_dim(steps, lax.axis_index("sp") * columns, columns, axis=1)
    mixed_heads = mixer(signal, write, read, conv_x, conv_b, conv_c, steps, decay_rate)
    mixed_tokens = to_tokens(sp_count, mixed_heads)

    token_count = residual_in.shape[1]
    model_width = residual_in.shape[2]
    gated = mixed_tokens.astype(f32) * jax.nn.silu(gate_input[0].astype(f32))
    mixed = group_scale(gated, mix_gain).astype(bf16)
    depth = out_weight.shape[0]
    me = lax.axis_index("dp")
    stream = residual_in[0].astype(f32)
    for offset, block in parts.items():
        piece = lax.dynamic_slice_in_dim(mixed, (me ^ offset) * depth, depth, axis=1)
        stream = stream + jnp.dot(piece, block, preferred_element_type=f32)
    ffn_input = scale_rows(stream, ffn_gain).astype(bf16)

    top_count = routing.shape[2]
    capacity = 2 * token_count * top_count // (sp_count * dp_count)
    flat = near * capacity
    earlier = (
        lax.iota(jnp.int32, token_count)[:, None] < lax.iota(jnp.int32, token_count)[None, :]
    ).astype(bf16)

    def tables(names, weights):
        chosen = names.T[:, None, :] == (first_expert + lax.iota(jnp.int32, near))[None, :, None]
        named = jnp.any(chosen, axis=0)
        weight_of = jnp.sum(jnp.where(chosen, weights.T[:, None, :], 0.0), axis=0)
        slot = jnp.dot(named.astype(bf16), earlier, preferred_element_type=f32).astype(jnp.int32)
        slot = jnp.where(named, slot, -1)
        pick = slot[:, None, :] == lax.iota(jnp.int32, capacity)[None, :, None]
        high = weight_of.astype(bf16)
        low = (weight_of - high.astype(f32)).astype(bf16)
        zero = jnp.zeros((), bf16)
        combine = jnp.concatenate(
            [
                jnp.where(pick, high[:, None, :], zero).reshape(flat, token_count),
                jnp.where(pick, low[:, None, :], zero).reshape(flat, token_count),
            ],
            axis=1,
        )
        return pick.astype(bf16).reshape(flat, token_count), combine

    def dispatch(select, tokens, identity):
        outgoing = jnp.dot(select, tokens, preferred_element_type=f32).astype(bf16)
        return swap_half(half, dp_count, outgoing.reshape(near, capacity, model_width), identity)

    def serve(arrived):
        return expert_apply(
            arrived.reshape(flat, model_width), gate_w[0], up_w[0], down_w[0]
        ).reshape(arrived.shape)

    def collect(combine, served, identity):
        returned = swap_half(half, dp_count, served, identity)
        sums = lax.dot_general(
            combine, returned.reshape(flat, model_width), (((0,), (0,)), ((), ())),
            preferred_element_type=f32,
        )
        return sums[:token_count] + sums[token_count:]

    select_own, combine_own = tables(routing[0], route_weight[0])
    select_far, combine_far = tables(far_routing, far_weight)
    far_input = lax.ppermute(ffn_input, "sp", mirror)
    arrived_own = dispatch(select_own, ffn_input, 3)
    arrived_far = dispatch(select_far, far_input, 4)
    part_far = collect(combine_far, serve(arrived_far), 5).astype(bf16)
    part_back = lax.ppermute(part_far, "sp", mirror)
    routed = collect(combine_own, serve(arrived_own), 6)
    return (stream + routed + part_back.astype(f32)).astype(bf16)[None]


def solution(mesh):
    return jax.shard_map(
        per_device,
        mesh=mesh,
        in_specs=(
            P("dp", "sp", None),
            P("dp", "sp", None),
            P("dp", "sp", None),
            P("dp", "sp", None),
            P("dp", "sp", None),
            P("dp", "sp", None),
            P(None, "sp"),
            P(None, "sp"),
            P(None, "sp"),
            P(None, "sp"),
            P(),
            P("dp", None),
            P(),
            P("dp", "sp", None),
            P("dp", "sp", None),
            P(("sp", "dp"), None, None),
            P(("sp", "dp"), None, None),
            P(("sp", "dp"), None, None),
        ),
        out_specs=P("dp", "sp", None),
        check_vma=False,
    )
```

time: 604 us -> 299 us (0.50)
  the two profiles are of different devices: /device:TPU:0 before, /device:TPU:7 now
where the time goes in v1:
time: 299 us
  Pallas kernels  225 us (75%)
  matrix products  51.8 us (17%)
  starting transfers between devices  9.67 us (3%)
  local copies, waits for them, and re-layouts  6.19 us (2%)
  other arithmetic  5.84 us (2%)
    pallas_call x4, Pallas kernels, swap_half(): pl.pallas_call(functools.partial(swap_half_kernel, half, dp_count), out_s...  159 us
    pallas_call x1, Pallas kernels, to_heads(): pl.pallas_call(functools.partial(to_heads_kernel, n), out_shape=(wide, wi...  36.1 us
    dot_general x2, matrix products, expert_apply(): jnp.dot(active, down_mat, preferred_element_type=jnp.float32)  21.4 us
    pallas_call x1, Pallas kernels, to_tokens(): pl.pallas_call(functools.partial(to_tokens_kernel, n), out_shape=jax.Shap...  21 us
    dot_general x2, matrix products, expert_apply(): jnp.dot(rows, up_mat, preferred_element_type=jnp.float32)  13.2 us
    pallas_call x1, Pallas kernels, mixer(): pl.pallas_call(mixer_kernel, grid=(groups,), out_shape=jax.ShapeDtypeStru...  8.71 us
    dot_general x4, matrix products, per_device(): stream = stream + jnp.dot(piece, block, preferred_element_type=f32)  8.25 us
  transfers between devices with their start and end apart: 7, of which 0 were waited for; matrix products, arithmetic and copies ran while one was open for 12% of the time, Pallas kernels for 52%

profile of v1, /device:TPU:7, one launch (start us, length us, event | category | flops | bytes accessed | tf_op | source)
XLA Modules:
  0.0 298.7 jit_solution(8774495545729705565)
XLA Ops:
  0.9 2.3 collective-permute-start.3
  4.2 1.4 copy.48
  5.7 36.1 %to_heads.1 = (bf16[1024,256]{1,0:T(8,128)(2,1)}, bf16[1024,256]{1,0:T(8,128)(2,1)}, bf16[1024,256]{1,0:T(8,128)(2,1)}, bf16[1024,64]{1,0:T(8,128)(2,1)}) custom-call(bf16[128,2048]{1,0:T(8,128)(2,1)} %bitcast.112, bf16[128,2048]{1,0:T(8,128)(2,1)} %bitcast.113, bf16[128,2048]{1,0:T(8,128)(2,1)} %bitcast.114, bf16[128,64]{1,0:T(8,128)(2,1)} %bitcast.115), custom_call_target="tpu_custom_call" | custom-call | tf_op jit(solution)/shard_map/to_heads/pallas_call | solution.py:81
  43.7 8.7 %mixer.1.src = bf16[1024,256]{1,0:T(8,128)(2,1)S(1)} custom-call(bf16[1024,256]{1,0:T(8,128)(2,1)S(1)} %copy-done.1, bf16[1024,256]{1,0:T(8,128)(2,1)S(1)} %copy-done.2, bf16[1024,256]{1,0:T(8,128)(2,1)S(1)} %copy-done.3, f32[7,256]{1,0:T(8,128)S(1)} %copy-done.4, f32[7,256]{1,0:T(8,128)S(1)} %copy-done.5, f32[7,256]{1,0:T(8,128)S(1)} %copy-done.6, ...), custom_call_target="tpu_custom_call" | custom-call | flops 40000000000 | bytes 2097152 | tf_op jit(solution)/shard_map/mixer/pallas_call | solution.py:353
  53.2 21.0 %to_tokens.1 = bf16[128,2048]{1,0:T(8,128)(2,1)} custom-call(bf16[1024,256]{1,0:T(8,128)(2,1)} %copy-done), custom_call_target="tpu_custom_call" | custom-call | tf_op jit(solution)/shard_map/to_tokens/pallas_call | solution.py:133
  74.2 1.4 fusion.55
  77.1 2.8 collective-permute-start.2
  80.4 2.0 convolution_add_fusion.2
  84.1 2.0 fusion.51
  86.2 2.0 fusion.18
  88.2 2.1 multiply_reduce_fusion
  92.9 2.0 convolution_convert_fusion.1
  94.9 44.3 %swap_half_3.1 = bf16[16,32,2048]{2,1,0:T(8,128)(2,1)} custom-call(bf16[16,32,2048]{2,1,0:T(8,128)(2,1)} %bitcast.111), custom_call_target="tpu_custom_call" | custom-call | flops 99999997952 | bytes 4194304 | tf_op jit(solution)/shard_map/swap_half_3/pallas_call | solution.py:200
  139.2 6.5 %fusion.10 = f32[512,1024]{1,0:T(8,128)} fusion(bf16[512,2048]{1,0:T(8,128)(2,1)} %bitcast.126, bf16[1,2048,1024]{2,1,0:T(8,128)(2,1)} %param.34), kind=kOutput, calls=%fused_computation.10 | convolution fusion | flops 2147483648 | bytes 8388608 | tf_op jit(solution)/shard_map/dot_general | solution.py:395
  145.8 11.0 %fusion.12 = bf16[512,2048]{1,0:T(8,128)(2,1)} fusion(bf16[1,1024,2048]{2,1,0:T(8,128)(2,1)} %param.35, f32[512,1024]{1,0:T(8,128)} %fusion.10, bf16[512,2048]{1,0:T(8,128)(2,1)} %bitcast.127, bf16[1,2048,1024]{2,1,0:T(8,128)(2,1)} %param.33), kind=kOutput, calls=%fused_computation.12 | convolution fusion | flops 4301258752 | bytes 14680064 | tf_op jit(solution)/shard_map/dot_general | solution.py:400
  156.7 2.0 convolution_convert_fusion
  158.8 34.6 %swap_half_4.1 = bf16[16,32,2048]{2,1,0:T(8,128)(2,1)} custom-call(bf16[16,32,2048]{2,1,0:T(8,128)(2,1)} %bitcast.110), custom_call_target="tpu_custom_call" | custom-call | flops 99999997952 | bytes 4194304 | tf_op jit(solution)/shard_map/swap_half_4/pallas_call | solution.py:200
  193.4 6.6 %fusion.8 = f32[512,1024]{1,0:T(8,128)} fusion(bf16[512,2048]{1,0:T(8,128)(2,1)} %bitcast.128, bf16[1,2048,1024]{2,1,0:T(8,128)(2,1)} %param.34), kind=kOutput, calls=%fused_computation.8 | convolution fusion | flops 2147483648 | bytes 8388608 | tf_op jit(solution)/shard_map/dot_general | solution.py:395
  200.1 10.4 %fusion.15 = bf16[512,2048]{1,0:T(8,128)(2,1)} fusion(bf16[1,1024,2048]{2,1,0:T(8,128)(2,1)} %param.35, f32[512,1024]{1,0:T(8,128)} %fusion.8, bf16[512,2048]{1,0:T(8,128)(2,1)S(1)} %bitcast.129, bf16[1,2048,1024]{2,1,0:T(8,128)(2,1)} %param.33), kind=kOutput, calls=%fused_computation.13 | convolution fusion | flops 4301258752 | bytes 14680064 | tf_op jit(solution)/shard_map/dot_general | solution.py:400
  210.5 34.7 %swap_half_5.1 = bf16[16,32,2048]{2,1,0:T(8,128)(2,1)} custom-call(bf16[16,32,2048]{2,1,0:T(8,128)(2,1)} %bitcast.130), custom_call_target="tpu_custom_call" | custom-call | flops 99999997952 | bytes 4194304 | tf_op jit(solution)/shard_map/swap_half_5/pallas_call | solution.py:200
  245.2 2.3 fusion.42
  247.7 2.3 collective-permute-start.6
  250.0 45.1 %swap_half_6.1 = bf16[16,32,2048]{2,1,0:T(8,128)(2,1)} custom-call(bf16[16,32,2048]{2,1,0:T(8,128)(2,1)} %bitcast.125), custom_call_target="tpu_custom_call" | custom-call | flops 99999997952 | bytes 4194304 | tf_op jit(solution)/shard_map/swap_half_6/pallas_call | solution.py:200
  295.1 2.4 fusion.38
  (80 shorter events, 11.8 us)
Async XLA Ops:
  0.0 84.1 %collective-permute-start.1 = (bf16[512,2048]{1,0:T(8,128)(2,1)}, bf16[512,2048]{1,0:T(8,128)(2,1)}, u32[]{:S(2)}, u32[]{:S(2)}) collective-permute-start(bf16[512,2048]{1,0:T(8,128)(2,1)} %param.29), channel_id=1, source_target_pairs={{0,1},{1,0},{2,3},{3,2},{4,5},{5,4},{6,7},{7,6},{8,9},{9,8},{10,11... | collective-permute-start | bytes 6291464 | tf_op jit(solution)/shard_map/ppermute | solution.py:409
  0.7 76.4 %collective-permute-start = (bf16[512,2048]{1,0:T(8,128)(2,1)}, bf16[512,2048]{1,0:T(8,128)(2,1)}, u32[]{:S(2)}, u32[]{:S(2)}) collective-permute-start(bf16[512,2048]{1,0:T(8,128)(2,1)} %param.29), channel_id=1, source_target_pairs={{0,2},{1,3},{2,0},{3,1},{4,6},{5,7},{6,4},{7,5},{8,10},{9,11},{10,... | collective-permute-start | bytes 6291464 | tf_op jit(solution)/shard_map/ppermute | solution.py:409
  0.9 81.7 %collective-permute-start.3 = (s32[128,4]{0,1:T(4,128)}, s32[128,4]{0,1:T(4,128)S(1)}, u32[]{:S(2)}, u32[]{:S(2)}) collective-permute-start(s32[128,4]{0,1:T(4,128)} %bitcast.116), channel_id=1, source_target_pairs={{0,16},{4,20},{8,24},{12,28},{16,0},{20,4},{24,8},{28,12},{1,17},{... | collective-permute-start | bytes 6152 | tf_op jit(solution)/shard_map/ppermute | solution.py:425
  3.2 79.9 %collective-permute-start.4 = (f32[128,4]{0,1:T(4,128)}, f32[128,4]{0,1:T(4,128)S(1)}, u32[]{:S(2)}, u32[]{:S(2)}) collective-permute-start(f32[128,4]{0,1:T(4,128)} %bitcast.121), channel_id=1, source_target_pairs={{0,16},{4,20},{8,24},{12,28},{16,0},{20,4},{24,8},{28,12},{1,17},{... | collective-permute-start | bytes 6152 | tf_op jit(solution)/shard_map/ppermute | solution.py:426
  3.3 40.3 %copy-start.4 = (f32[7,256]{1,0:T(8,128)S(1)}, f32[7,256]{1,0:T(8,128)}, u32[]{:S(2)}) copy-start(f32[7,256]{1,0:T(8,128)} %tx_ref.1) | copy-start | bytes 21508
  3.3 40.3 %copy-start.5 = (f32[7,256]{1,0:T(8,128)S(1)}, f32[7,256]{1,0:T(8,128)}, u32[]{:S(2)}) copy-start(f32[7,256]{1,0:T(8,128)} %tb_ref.1) | copy-start | bytes 21508
  3.3 40.3 %copy-start.6 = (f32[7,256]{1,0:T(8,128)S(1)}, f32[7,256]{1,0:T(8,128)}, u32[]{:S(2)}) copy-start(f32[7,256]{1,0:T(8,128)} %tc_ref.1) | copy-start | bytes 21508
  41.8 1.8 copy-start.1
  43.6 30.5 %copy-start.10 = (bf16[1,128,2048]{2,1,0:T(8,128)(2,1)S(1)}, bf16[1,128,2048]{2,1,0:T(8,128)(2,1)}, u32[]{:S(2)}) copy-start(bf16[1,128,2048]{2,1,0:T(8,128)(2,1)} %param.23) | copy-start | bytes 1572868
  76.3 3.7 %copy-start.9 = (bf16[128,2048]{1,0:T(8,128)(2,1)S(1)}, bf16[128,2048]{1,0:T(8,128)(2,1)}, u32[]{:S(2)}) copy-start(bf16[128,2048]{1,0:T(8,128)(2,1)} %to_tokens.1) | copy-start | bytes 1572868
  76.3 3.7 %copy-start.16 = (f32[2048]{0:T(1024)S(1)}, f32[2048]{0:T(1024)}, u32[]{:S(2)}) copy-start(f32[2048]{0:T(1024)} %param.28) | copy-start | bytes 24580
  76.7 3.7 %copy-start.15 = (bf16[1,128,2048]{2,1,0:T(8,128)(2,1)S(1)}, bf16[1,128,2048]{2,1,0:T(8,128)(2,1)}, u32[]{:S(2)}) copy-start(bf16[1,128,2048]{2,1,0:T(8,128)(2,1)} %param.18) | copy-start | bytes 1572868
  77.1 11.1 %collective-permute-start.2 = (bf16[512,2048]{1,0:T(8,128)(2,1)}, bf16[512,2048]{1,0:T(8,128)(2,1)}, u32[]{:S(2)}, u32[]{:S(2)}) collective-permute-start(bf16[512,2048]{1,0:T(8,128)(2,1)} %collective-permute-done), channel_id=1, source_target_pairs={{0,1},{1,0},{2,3},{3,2},{4,5},{5,4},{6,7},{7,6},{8,9},{9,8},{10,11... | collective-permute-start | bytes 6291464 | tf_op jit(solution)/shard_map/ppermute | solution.py:409
  80.4 2.2 copy-start.18
  80.4 2.7 copy-start.19
  88.2 3.2 %copy-start.17 = (f32[2048]{0:T(1024)S(1)}, f32[2048]{0:T(1024)}, u32[]{:S(2)}) copy-start(f32[2048]{0:T(1024)} %param.30) | copy-start | bytes 24580
  91.6 65.1 %collective-permute-start.5 = (bf16[128,2048]{1,0:T(8,128)(2,1)S(1)}, bf16[128,2048]{1,0:T(8,128)(2,1)S(1)}, u32[]{:S(2)}, u32[]{:S(2)}) collective-permute-start(bf16[128,2048]{1,0:T(8,128)(2,1)S(1)} %multiply_convert_fusion.2), channel_id=1, source_target_pairs={{0,16},{4,20},{8,24},{12,28},{16,0},{20,4},{24,8},{28,12},{1,17},{... | collective-permute-start | bytes 1572872 | tf_op jit(solution)/shard_map/ppermute | solution.py:493
  193.4 6.7 %copy-start.20 = (bf16[16,32,2048]{2,1,0:T(8,128)(2,1)S(1)}, bf16[16,32,2048]{2,1,0:T(8,128)(2,1)}, u32[]{:S(2)}) copy-start(bf16[16,32,2048]{2,1,0:T(8,128)(2,1)} %swap_half_4.1) | copy-start | bytes 6291460
  210.5 34.8 %copy-start.13 = (bf16[512,128]{1,0:T(8,128)(2,1)S(1)}, bf16[512,128]{1,0:T(8,128)(2,1)}, u32[]{:S(2)}) copy-start(bf16[512,128]{1,0:T(8,128)(2,1)} %get-tuple-element.25) | copy-start | bytes 393220
  210.5 34.8 %copy-start.14 = (bf16[512,128]{1,0:T(8,128)(2,1)S(1)}, bf16[512,128]{1,0:T(8,128)(2,1)}, u32[]{:S(2)}) copy-start(bf16[512,128]{1,0:T(8,128)(2,1)} %get-tuple-element.26) | copy-start | bytes 393220
  247.7 49.9 %collective-permute-start.6 = (bf16[128,2048]{1,0:T(8,128)(2,1)S(1)}, bf16[128,2048]{1,0:T(8,128)(2,1)S(1)}, u32[]{:S(2)}, u32[]{:S(2)}) collective-permute-start(bf16[128,2048]{1,0:T(8,128)(2,1)S(1)} %fusion.29), channel_id=1, source_target_pairs={{0,16},{4,20},{8,24},{12,28},{16,0},{20,4},{24,8},{28,12},{1,17},{... | collective-permute-start | bytes 1572872 | tf_op jit(solution)/shard_map/ppermute | solution.py:497
  250.0 45.2 %copy-start.11 = (bf16[512,128]{1,0:T(8,128)(2,1)S(1)}, bf16[512,128]{1,0:T(8,128)(2,1)}, u32[]{:S(2)}) copy-start(bf16[512,128]{1,0:T(8,128)(2,1)} %get-tuple-element.21) | copy-start | bytes 393220
  250.0 45.2 %copy-start.12 = (bf16[512,128]{1,0:T(8,128)(2,1)S(1)}, bf16[512,128]{1,0:T(8,128)(2,1)}, u32[]{:S(2)}) copy-start(bf16[512,128]{1,0:T(8,128)(2,1)} %get-tuple-element.22) | copy-start | bytes 393220
  295.1 2.4 copy-start.8
  (4 other events, 5.5 us)
